TPU v7x, 32 devices: a whole 2x2x4 slice. The times are simulated.
32 devices in a mesh: sp: 8 (over z, y), tp: 4 (over x, core).
Axes of the slice: x: 2, y: 2, z: 4, core: 2. Of those that a mesh axis runs over, the one named last changes fastest.
Arguments:
- memory_queries: bfloat16 [4096, 1024], P('sp', 'tp'), may hold values from -8 to 8
- memory_keys: bfloat16 [4096, 1024], P('sp', 'tp'), may hold values from -8 to 8
- memory_values: bfloat16 [4096, 1024], P('sp', 'tp'), may hold values from -6 to 6
- input_gate_logits: float32 [8, 4096], P('tp', 'sp'), may hold values from -64 to 160
- forget_gate_logits: float32 [8, 4096], P('tp', 'sp'), may hold values from -0.1 to 20
- extra_log_decay: float32 [8, 4096], P('tp', 'sp'), may hold values from -1.4 to 0
- residual: bfloat16 [4096, 2048], P(('sp', 'tp')), may hold values from -6 to 6
- cell_output_weight: bfloat16 [1024, 2048], P('tp', 'sp'), may hold values from -0.1875 to 0.1875
- expert_norm_gain: float32 [2048], replicated, may hold values from 0.1 to 1.9
- expert_gate_weight: bfloat16 [8, 2048, 3584], P('sp', None, 'tp'), may hold values from -0.125 to 0.125
- expert_up_weight: bfloat16 [8, 2048, 3584], P('sp', None, 'tp'), may hold values from -0.125 to 0.125
- expert_down_weight: bfloat16 [8, 3584, 2048], P('sp', 'tp'), may hold values from -0.09375 to 0.09375
- routed_expert_index: int32 [4096, 2], P('sp'), may hold values from 0 to 7, as said below
- routed_expert_weight: float32 [4096, 2], P(('sp', 'tp')), may hold values from 0.1 to 1
Outputs:
- layer_out: bfloat16 [4096, 2048], P(('sp', 'tp'))
Inputs may be any that keep to these rules, and one draw needn't show every extreme that they name: `routed_expert_index`: each row names 2 different experts. In each aligned block of 128 rows (the rows of one device after the cell) no expert is named more than 40 times, and one expert is named exactly 40 times in every block.
All inputs are finite; a program needn't handle non-finite values.
Results may differ from a plain program's by a relative error of at most 0.013.
Values may be sent and summed in bfloat16 or wider, within the bound.
A program may use at most 128 MiB of HBM per device.

v0:
```python
import jax
import jax.numpy as jnp
from jax import lax
from jax.sharding import PartitionSpec as P

highest = lax.Precision.HIGHEST
lowest = -1e30
epsilon = 1e-06


def carried_in(x, axis, combine, identity):
    length, place = (lax.axis_size(axis), lax.axis_index(axis))
    everything = jax.tree.map(lambda part: lax.all_gather(part, axis), x)
    start = jax.tree.map(
        lambda part, zero: jnp.broadcast_to(jnp.asarray(zero, part.dtype), part.shape), x, identity
    )

    def turn(k, before):
        reached = k < place
        new = combine(before, jax.tree.map(lambda part: part[k], everything))
        return jax.tree.map(lambda a, b: jnp.where(reached, a, b), new, before)

    return lax.fori_loop(0, length, turn, start)


def block_pass(memory, inputs):
    state_mat, state_norm, state_max = memory
    queries, keys_blk, values_blk, gate_in, forget_log_value = inputs
    length = gate_in.shape[-1]
    running = jnp.cumsum(forget_log_value, axis=-1)
    causal = jnp.arange(length)[:, None] >= jnp.arange(length)[None, :]
    exponent = running[:, :, None] - running[:, None, :] + gate_in[:, None, :]
    exponent = jnp.where(causal[None], exponent, -jnp.inf)
    carried = running + state_max[:, None]
    row_max = jnp.maximum(carried, jnp.max(exponent, axis=-1))
    decays = jnp.exp(exponent - row_max[:, :, None])
    carry_scale = jnp.exp(carried - row_max)
    dispatch_affinity = jnp.einsum("htk,hsk->hts", queries, keys_blk, precision=highest) * decays
    numerator = carry_scale[:, :, None] * jnp.einsum(
        "hvk,htk->htv", state_mat, queries, precision=highest
    )
    numerator = numerator + jnp.einsum(
        "hts,hsv->htv", dispatch_affinity, values_blk, precision=highest
    )
    denominator = carry_scale * jnp.einsum(
        "hk,htk->ht", state_norm, queries, precision=highest
    ) + jnp.sum(dispatch_affinity, axis=-1)
    final_log = running[:, -1]
    log_prev = final_log + state_max
    log_keep = final_log[:, None] - running + gate_in
    new_max = jnp.maximum(log_prev, jnp.max(log_keep, axis=-1))
    prev_scale = jnp.exp(log_prev - new_max)
    retain = jnp.exp(log_keep - new_max[:, None])
    new_mat = prev_scale[:, None, None] * state_mat + jnp.einsum(
        "hsv,hsk->hvk", retain[:, :, None] * values_blk, keys_blk, precision=highest
    )
    new_norm = prev_scale[:, None] * state_norm + jnp.einsum(
        "hs,hsk->hk", retain, keys_blk, precision=highest
    )
    return ((new_mat, new_norm, new_max), (numerator, denominator, row_max))


def join_states(earlier, later):
    early_log, early_mat, early_norm, early_max = earlier
    late_log, late_mat, late_norm, late_max = later
    joined_max = jnp.maximum(early_max + late_log, late_max)
    early_scale = jnp.exp(early_max + late_log - joined_max)
    late_scale = jnp.exp(late_max - joined_max)
    joined_mat = early_scale[:, None, None] * early_mat + late_scale[:, None, None] * late_mat
    joined_norm = early_scale[:, None] * early_norm + late_scale[:, None] * late_norm
    return (early_log + late_log, joined_mat, joined_norm, joined_max)


def matrix_memory_step(
    memory_queries,
    memory_keys,
    memory_values,
    input_gate_logits,
    forget_gate_logits,
    extra_log_decay,
):
    tokens_here, channels = memory_queries.shape
    heads_here = input_gate_logits.shape[0]
    head_dim = channels // heads_here

    def heads_first(tensor):
        return jnp.transpose(
            tensor.astype(jnp.float32).reshape(tokens_here, heads_here, head_dim), (1, 0, 2)
        )

    queries = heads_first(memory_queries) * head_dim ** (-0.5)
    forget_log_value = jax.nn.log_sigmoid(forget_gate_logits) + extra_log_decay
    block_size = min(tokens_here, 256)
    block_count = tokens_here // block_size

    def split_blocks(tensor):
        return jnp.moveaxis(
            tensor.reshape((heads_here, block_count, block_size) + tensor.shape[2:]), 1, 0
        )

    def join_blocks(tensor):
        return jnp.moveaxis(tensor, 0, 1).reshape((heads_here, tokens_here) + tensor.shape[3:])

    empty_state = (
        jnp.zeros((heads_here, head_dim, head_dim), jnp.float32),
        jnp.zeros((heads_here, head_dim), jnp.float32),
        jnp.full((heads_here,), lowest, jnp.float32),
    )
    members = (
        queries,
        heads_first(memory_keys),
        heads_first(memory_values),
        input_gate_logits,
        forget_log_value,
    )
    end_state, pieces = lax.scan(
        block_pass, empty_state, tuple((split_blocks(member) for member in members))
    )
    numerator, denominator, row_max = (join_blocks(member) for member in pieces)
    running = jnp.cumsum(forget_log_value, axis=-1)
    identity = (jnp.zeros((heads_here,), jnp.float32),) + empty_state
    incoming = carried_in((running[:, -1],) + tuple(end_state), "sp", join_states, identity)
    prior_mat, prior_norm, prior_max = incoming[1:]
    reached = running + prior_max[:, None]
    joined = jnp.maximum(row_max, reached)
    local_scale = jnp.exp(row_max - joined)
    carry_scale = jnp.exp(reached - joined)
    numerator = local_scale[:, :, None] * numerator + carry_scale[:, :, None] * jnp.einsum(
        "hvk,htk->htv", prior_mat, queries, precision=highest
    )
    denominator = local_scale * denominator + carry_scale * jnp.einsum(
        "hk,htk->ht", prior_norm, queries, precision=highest
    )
    guarded = jnp.maximum(jnp.abs(denominator), jnp.exp(-joined))
    return ((numerator / guarded[:, :, None]).astype(jnp.bfloat16), heads_here, head_dim)


def slot_index(ids, experts, capacity):
    flat_ids = ids.reshape(-1)
    matches = (flat_ids[:, None] == jnp.arange(experts, dtype=jnp.int32)[None, :]).astype(jnp.int32)
    before = jnp.cumsum(matches, axis=0) - matches
    return flat_ids * capacity + jnp.sum(before * matches, axis=1)


def local(
    memory_queries,
    memory_keys,
    memory_values,
    input_gate_logits,
    forget_gate_logits,
    extra_log_decay,
    residual,
    cell_output_weight,
    expert_norm_gain,
    expert_gate_weight,
    expert_up_weight,
    expert_down_weight,
    routed_expert_index,
    routed_expert_weight,
):
    hidden, heads_here, head_dim = matrix_memory_step(
        memory_queries,
        memory_keys,
        memory_values,
        input_gate_logits,
        forget_gate_logits,
        extra_log_decay,
    )
    weight_piece = lax.all_gather(cell_output_weight, "sp", axis=1, tiled=True)
    shaped = weight_piece.reshape(heads_here, head_dim, weight_piece.shape[1])
    partial_rows = jnp.einsum(
        "htd,hdc->tc", hidden, shaped, preferred_element_type=jnp.float32
    ).astype(jnp.bfloat16)
    projected = lax.psum_scatter(
        partial_rows.astype(jnp.float32).astype(jnp.bfloat16), "tp", scatter_dimension=0, tiled=True
    ).astype(jnp.float32)
    mixed_rows = (residual.astype(jnp.float32) + projected).astype(jnp.bfloat16)
    mixed_wide = mixed_rows.astype(jnp.float32)
    norm_scale = lax.rsqrt(jnp.mean(mixed_wide * mixed_wide, axis=-1, keepdims=True) + epsilon)
    normed = (mixed_wide * norm_scale * expert_norm_gain).astype(jnp.bfloat16)
    sp_size = lax.axis_size("sp")
    row_count, model_width = residual.shape
    top_count = routed_expert_index.shape[1]
    experts = sp_size * expert_gate_weight.shape[0]
    assigned = row_count * top_count
    capacity = max(2, assigned * 5 // (4 * experts))
    own_ids = lax.dynamic_slice_in_dim(
        routed_expert_index, lax.axis_index("tp") * row_count, row_count, 0
    )
    own_slots = slot_index(own_ids, experts, capacity)
    zero_row = jnp.zeros((1, model_width), jnp.bfloat16)
    padded = jnp.concatenate([normed, zero_row], axis=0)
    slot_table = jnp.full((experts * capacity,), row_count, jnp.int32)
    slot_table = slot_table.at[own_slots].set(jnp.arange(assigned, dtype=jnp.int32) // top_count)
    arrived = lax.all_gather(
        lax.all_to_all(
            padded[slot_table.reshape(experts, 1, capacity)],
            "sp",
            split_axis=0,
            concat_axis=0,
            tiled=True,
        ),
        "tp",
        axis=1,
        tiled=True,
    )
    sources, owners, slot_span, width_in = arrived.shape
    flat_rows = arrived.reshape(-1, width_in)
    gate_pre = jnp.dot(flat_rows, expert_gate_weight[0], preferred_element_type=jnp.float32)
    up_pre = jnp.dot(flat_rows, expert_up_weight[0], preferred_element_type=jnp.float32)
    hidden_act = (jax.nn.silu(gate_pre) * up_pre).astype(jnp.bfloat16)
    group_term = jnp.dot(hidden_act, expert_down_weight[0], preferred_element_type=jnp.float32)
    group_term = lax.optimization_barrier(group_term.astype(jnp.bfloat16)).astype(jnp.float32)
    summed = lax.psum_scatter(
        group_term.reshape(sources, owners, slot_span, width_in).astype(jnp.bfloat16),
        "tp",
        scatter_dimension=1,
        tiled=True,
    )
    returned = lax.all_to_all(summed, "sp", split_axis=0, concat_axis=0, tiled=True)
    picked = returned.reshape(experts * capacity, model_width)[own_slots]
    picked = picked.reshape(row_count, top_count, model_width).astype(jnp.float32)
    routed_sum = jnp.sum(picked * routed_expert_weight[:, :, None], axis=1)
    return (mixed_wide + routed_sum).astype(jnp.bfloat16)


def solution(mesh):
    return jax.shard_map(
        local,
        mesh=mesh,
        in_specs=(
            P("sp", "tp"),
            P("sp", "tp"),
            P("sp", "tp"),
            P("tp", "sp"),
            P("tp", "sp"),
            P("tp", "sp"),
            P(("sp", "tp"), None),
            P("tp", "sp"),
            P(),
            P("sp", None, "tp"),
            P("sp", None, "tp"),
            P("sp", "tp", None),
            P("sp", None),
            P(("sp", "tp"), None),
        ),
        out_specs=P(("sp", "tp"), None),
        check_vma=False,
    )
```

profile of v0, /device:TPU:0, one launch (start us, length us, event | category | flops | bytes accessed | tf_op | source)
XLA Modules:
  0.0 404.9 jit_solution(8255470432722626242)
XLA Ops:
  6.6 1.1 copy.56
  7.8 0.2 copy.57
  8.0 1.1 copy.54
  9.9 11.3 %while.39 = (s32[]{:T(128)}, f32[2,128,128]{2,1,0:T(8,128)S(1)}, f32[2,128]{1,0:T(2,128)S(1)}, f32[2]{0:T(128)S(1)}, f32[2,2,256,128]{3,2,0,1:T(8,128)S(1)}, /*i...) while((s32[]{:T(128)}, f32[2,128,128]{2,1,0:T(8,128)S(1)}, ...), condition=%wide.region_6.7_spmd.clone, body=%wide.region_0.6_spmd.clone.sunk | while | flops 607329536 | bytes 4625314 | solution.py:116
  9.9 0.6 reduce-window.38
  11.4 0.2 fusion.122
  11.7 0.6 fusion.123
  12.4 0.2 fusion.121
  12.7 0.3 fusion.124
  13.3 0.4 convolution_multiply_fusion.4
  13.6 1.0 fusion.125
  14.8 0.7 convolution_add_fusion.3
  15.6 0.6 reduce-window.38
  17.0 0.2 fusion.122
  17.3 0.6 fusion.123
  18.0 0.2 fusion.121
  18.4 0.3 fusion.124
  18.9 0.4 convolution_multiply_fusion.4
  19.3 1.0 fusion.125
  20.4 0.7 convolution_add_fusion.3
  21.2 0.6 copy-done
  21.9 0.7 all-gather.9.cloned.1.call-update
  22.7 0.6 reduce-window.22
  23.9 0.7 dynamic-slice
  25.3 0.2 dynamic-update-slice.1
  25.6 23.2 %all-reduce.4 = (f32[16]{0:T(128)S(1)}, f32[16]{0:T(128)S(1)}) all-reduce(f32[16]{0:T(128)S(1)} %bitcast_dynamic-update-slice_fusion.1, f32[16]{0:T(128)S(1)} %dynamic-update-slice.1), channel_id=2, replica_groups=mesh['sp'=8,'tp'=4] {'sp'}, use_global_device_ids=true, to_apply=%add.1 | all-reduce | flops 32 | bytes 256
  49.0 16.4 %all-gather.4 = f32[8,2,128]{2,1,0:T(2,128)S(1)} all-gather(f32[1,2,128]{2,1,0:T(2,128)S(1)} %bitcast.293), channel_id=5, replica_groups=mesh['sp'=8,'tp'=4] {'sp'}, dimensions={0}, use_global_device_ids=true | all-gather | bytes 9216 | tf_op jit(solution)/shard_map/all_gather | solution.py:13
  65.4 9.0 %while.40 = (s32[]{:T(128)}, f32[2,128,128]{2,1,0:T(8,128)S(1)}, f32[2,128]{1,0:T(2,128)S(1)}, f32[2]{0:T(128)S(1)}, s32[]{:T(128)}, /*index=5*/f32[8,2]{1,0:T(8...) while((s32[]{:T(128)}, f32[2,128,128]{2,1,0:T(8,128)S(1)}, ...), condition=%wide.region_10.11_spmd.clone, body=%wide.region_9.10_spmd.clone.sunk | while | flops 165138 | bytes 396541 | solution.py:23
  65.5 1.0 fusion.126
  66.6 1.0 fusion.126
  67.7 1.0 fusion.126
  68.8 1.0 fusion.126
  69.9 1.0 fusion.126
  71.1 1.0 fusion.126
  72.2 1.0 fusion.126
  73.3 1.0 fusion.126
  74.4 0.4 fusion.66
  74.9 0.2 bitcast_multiply_fusion.5
  75.1 1.2 fusion.47
  76.3 29.1 %all-gather.9.cloned.1.call-done = bf16[256,2048]{1,0:T(8,128)(2,1)} async-done(((bf16[256,256]{1,0:T(8,128)(2,1)}), bf16[256,2048]{1,0:T(8,128)(2,1)}) %all-gather.9.cloned.1.call-update) | async-done | bytes 1048592 | tf_op jit(solution)/shard_map/all_gather | solution.py:169
  105.3 3.3 bitcast_convert_fusion
  108.7 0.7 broadcast_multiply_fusion
  109.8 0.6 reduce-window.26
  110.4 0.2 slice_reduce_fusion.2
  111.0 1.4 scatter_custom_fusion
  112.6 26.4 %reduce-scatter.3.cloned.1.call-done = bf16[128,2048]{1,0:T(8,128)(2,1)} async-done(((bf16[512,2048]{1,0:T(8,128)(2,1)}), bf16[128,2048]{1,0:T(8,128)(2,1)}) %reduce-scatter.3.cloned.1.call-update) | async-done | bytes 524304 | tf_op jit(solution)/shard_map/reduce_scatter | solution.py:174
  139.0 1.3 fusion.48
  140.3 1.3 fusion.50
  141.6 2.4 gather_fusion
  144.0 36.6 %all_to_all.10 = bf16[8,1,40,2048]{3,2,1,0:T(8,128)(2,1)} all-to-all(bf16[8,1,40,2048]{3,2,1,0:T(8,128)(2,1)S(1)} %bitcast.275), channel_id=1, replica_groups=mesh['sp'=8,'tp'=4] {'sp'}, dimensions={0} | all-to-all | bytes 2621440 | tf_op jit(solution)/shard_map/all_to_all | solution.py:196
  180.7 0.2 all-reduce.7.cloned.1.call-start
  180.9 38.4 %all-gather.11.cloned.1.call-done = bf16[8,4,40,2048]{3,2,1,0:T(8,128)(2,1)} async-done(((bf16[8,1,40,2048]{3,2,1,0:T(8,128)(2,1)}), bf16[8,4,40,2048]{3,2,1,0:T(8,128)(2,1)}) %all-gather.11.cloned.1.call-update) | async-done | bytes 5242896 | tf_op jit(solution)/shard_map/all_gather | solution.py:195
  219.3 10.0 %fusion.43 = f32[1280,896]{1,0:T(8,128)} fusion(bf16[1280,2048]{1,0:T(8,128)(2,1)} %bitcast.302, bf16[1,2048,896]{2,1,0:T(8,128)(2,1)} %param.27), kind=kOutput, calls=%fused_computation.81 | convolution fusion | flops 4697620480 | bytes 13500416 | tf_op jit(solution)/shard_map/dot_general | solution.py:209
  229.3 17.6 %convolution_convert_fusion = bf16[1280,2048]{1,0:T(8,128)(2,1)} fusion(bf16[1,896,2048]{2,1,0:T(8,128)(2,1)} %param.29, f32[1280,896]{1,0:T(8,128)} %fusion.43, bf16[1280,2048]{1,0:T(8,128)(2,1)} %bitcast.303, bf16[1,2048,896]{2,1,0:T(8,128)(2,1)} %param.28), kind=kOutput, calls=%fused_computation.76 | convolution fusion | flops 9404743680 | bytes 22413312 | tf_op jit(solution)/shard_map/dot_general | solution.py:212
  246.9 0.6 copy-done.9
  247.5 0.6 dynamic-slice.2
  248.1 101.5 %all-reduce.7.cloned.1.call-done = bf16[8,4,40,2048]{3,2,1,0:T(8,128)(2,1)} async-done(((bf16[8,4,40,2048]{3,2,1,0:T(8,128)(2,1)}), bf16[8,4,40,2048]{3,2,1,0:T(8,128)(2,1)}) %all-reduce.7.cloned.1.call-update) | async-done | bytes 5242896
  349.6 3.2 constant_dynamic-slice_fusion.3
  352.8 5.5 %all-to-all-start.1 = ((bf16[8,1,40,2048]{3,2,1,0:T(8,128)(2,1)}), bf16[8,1,40,2048]{3,2,1,0:T(8,128)(2,1)S(1)}, u32[]{:S(2)}, u32[]{:S(2)}) async-start(bf16[8,1,40,2048]{3,2,1,0:T(8,128)(2,1)} %constant_dynamic-slice_fusion.3), calls=%async_computation.2 | async-start | bytes 2621440 | tf_op jit(solution)/shard_map/all_to_all | solution.py:220
  358.5 30.9 %all-to-all-done.1 = bf16[8,1,40,2048]{3,2,1,0:T(8,128)(2,1)S(1)} async-done(((bf16[8,1,40,2048]{3,2,1,0:T(8,128)(2,1)}), bf16[8,1,40,2048]{3,2,1,0:T(8,128)(2,1)S(1)}, u32[]{:S(2)}, u32[]{:S(2)}) %all-to-all-start.1) | async-done | bytes 1310752 | tf_op jit(solution)/shard_map/all_to_all | solution.py:220
  389.4 2.3 gather_fusion.1
  391.7 2.4 reshape.428
  394.2 3.2 multiply_reduce_fusion
  397.3 1.0 fusion.51
  (137 shorter events, 6.6 us)
Async XLA Ops:
  6.5 2.9 copy-start.3
  6.5 3.3 copy-start.7
  6.5 3.3 copy-start.6
  6.5 3.3 copy-start.4
  6.5 58.9 %all-gather.13.cloned.1.call-start = ((), (), s32[]{:S(2)}) async-start(), calls=%async_computation.6 | async-start | bytes 1179648 | tf_op jit(solution)/shard_map/all_gather | solution.py:13
  9.9 14.0 %copy-start.10 = (u32[32]{0:T(128)S(1)}, u32[32]{0:T(128)}, u32[]{:S(2)}) copy-start(u32[32]{0:T(128)} %constant.125) | copy-start | bytes 388
  21.2 0.7 copy-start
  21.8 83.5 %all-gather.9.cloned.1.call-start = ((), (), s32[]{:S(2)}) async-start(), calls=%async_computation.3 | async-start | bytes 1179648 | tf_op jit(solution)/shard_map/all_gather | solution.py:169
  22.6 116.4 %reduce-scatter.3.cloned.1.call-start = ((), (), s32[]{:S(2)}) async-start(), calls=%async_computation.4 | async-start | bytes 2621440 | tf_op jit(solution)/shard_map/reduce_scatter | solution.py:174
  75.1 63.9 %copy-start.1 = (bf16[128,2048]{1,0:T(8,128)(2,1)S(1)}, bf16[128,2048]{1,0:T(8,128)(2,1)}, u32[]{:S(2)}) copy-start(bf16[128,2048]{1,0:T(8,128)(2,1)} %param.24) | copy-start | bytes 1572868
  76.2 64.0 %copy-start.5 = (f32[2048]{0:T(1024)S(1)}, f32[2048]{0:T(1024)}, u32[]{:S(2)}) copy-start(f32[2048]{0:T(1024)} %param.26) | copy-start | bytes 24580
  108.6 110.7 %all-gather.11.cloned.1.call-start = ((), (), s32[]{:S(2)}) async-start(), calls=%async_computation.5 | async-start | bytes 6553600 | tf_op jit(solution)/shard_map/all_gather | solution.py:195
  180.7 168.9 %all-reduce.7.cloned.1.call-start = ((), (), s32[]{:S(2)}) async-start(), calls=%async_computation.7 | async-start | bytes 10485760
  246.9 0.7 copy-start.9
  246.9 111.4 %copy-start.8 = (f32[128,2]{0,1:T(2,128)S(1)}, f32[128,2]{0,1:T(2,128)}, u32[]{:S(2)}) copy-start(f32[128,2]{0,1:T(2,128)} %param.31) | copy-start | bytes 3076
  352.8 36.5 %all-to-all-start.1 = ((bf16[8,1,40,2048]{3,2,1,0:T(8,128)(2,1)}), bf16[8,1,40,2048]{3,2,1,0:T(8,128)(2,1)S(1)}, u32[]{:S(2)}, u32[]{:S(2)}) async-start(bf16[8,1,40,2048]{3,2,1,0:T(8,128)(2,1)} %constant_dynamic-slice_fusion.3), calls=%async_computation.2 | async-start | bytes 2621440 | tf_op jit(solution)/shard_map/all_to_all | solution.py:220
  391.7 5.6 %copy-start.2 = (bf16[128,2048]{1,0:T(8,128)(2,1)S(1)}, bf16[128,2048]{1,0:T(8,128)(2,1)}, u32[]{:S(2)}) copy-start(bf16[128,2048]{1,0:T(8,128)(2,1)} %reduce-scatter.3.cloned.1.call-done) | copy-start | bytes 1572868
Sparse Core Ops, SparseCore 0:
  22.0 43.1 all-gather.12
  67.2 38.0 all-gather.8
  108.8 30.1 reduce-scatter.2
  180.8 38.4 all-gather.10
  247.0 102.5 all-reduce.6
where the time goes:
time: 406 us; the launch traced here: 405 us
  waiting for transfers between devices  227 us (56%)
  blocking collectives  76.3 us (19%)
  matrix products  39.1 us (10%)
  other arithmetic  22 us (5%)
  local copies, waits for them, and re-layouts  20.1 us (5%)
  between operations  14.2 us (3%)
  starting transfers between devices  5.89 us (1%)
    unnamed x6, waiting for transfers between devices  102 us
    all_gather x1, waiting for transfers between devices, local(): lax.all_gather(lax.all_to_all(padded[slot_table.reshape(experts, 1, capac...  38.4 us
    all_to_all x1, blocking collectives, local(): lax.all_to_all(padded[slot_table.reshape(experts, 1, capacity)], 'sp', sp...  36.6 us
    all_to_all x1, waiting for transfers between devices, local(): lax.all_to_all(summed, 'sp', split_axis=0, concat_axis=0, tiled=True)  30.9 us
    all_gather x1, waiting for transfers between devices, local(): weight_piece = lax.all_gather(cell_output_weight, 'sp', axis=1, tiled=True)  29.1 us
    reduce_scatter x1, waiting for transfers between devices, local(): lax.psum_scatter(partial_rows.astype(jnp.float32).astype(jnp.bfloat16), '...  26.4 us
    unnamed x1, blocking collectives  23.2 us
    dot_general x1, matrix products, local(): jnp.dot(hidden_act, expert_down_weight[0], preferred_element_type=jnp.flo...  17.6 us
  transfers between devices with their start and end apart: 6, of which 5 were waited for; matrix products, arithmetic and copies ran while one was open for 4% of the time, Pallas kernels for 0%

commit v1 on v0

--- a/solution.py
+++ b/solution.py
@@ -166,7 +166,7 @@
         forget_gate_logits,
         extra_log_decay,
     )
-    weight_piece = lax.all_gather(cell_output_weight, "sp", axis=1, tiled=True)
+    weight_piece = jnp.concatenate(lax.all_gather(cell_output_weight, "sp"), axis=1)
     shaped = weight_piece.reshape(heads_here, head_dim, weight_piece.shape[1])
     partial_rows = jnp.einsum(
         "htd,hdc->tc", hidden, shaped, preferred_element_type=jnp.float32

time: 406 us -> 409 us (level)
    unnamed x35 -> x39, local copies, waits for them, and re-layouts: 8.66 us -> 8.64 us
where the time goes in v1:
time: 409 us; the launch traced here: 408 us
  waiting for transfers between devices  229 us (56%)
  blocking collectives  76.3 us (19%)
  matrix products  37.9 us (9%)
  local copies, waits for them, and re-layouts  22.6 us (6%)
  other arithmetic  22 us (5%)
  between operations  14.2 us (3%)
  starting transfers between devices  5.71 us (1%)
    unnamed x6, waiting for transfers between devices  102 us
    all_gather x1, waiting for transfers between devices, local(): lax.all_gather(lax.all_to_all(padded[slot_table.reshape(experts, 1, capac...  38.6 us
    all_to_all x1, blocking collectives, local(): lax.all_to_all(padded[slot_table.reshape(experts, 1, capacity)], 'sp', sp...  36.6 us
    all_gather x1, waiting for transfers between devices, local(): lax.all_gather(cell_output_weight, 'sp')  31.4 us
    all_to_all x1, waiting for transfers between devices, local(): lax.all_to_all(summed, 'sp', split_axis=0, concat_axis=0, tiled=True)  30.9 us
    reduce_scatter x1, waiting for transfers between devices, local(): lax.psum_scatter(partial_rows.astype(jnp.float32).astype(jnp.bfloat16), '...  25.9 us
    unnamed x1, blocking collectives  23.3 us
    dot_general x1, matrix products, local(): jnp.dot(hidden_act, expert_down_weight[0], preferred_element_type=jnp.flo...  17.6 us
  transfers between devices with their start and end apart: 6, of which 5 were waited for; matrix products, arithmetic and copies ran while one was open for 4% of the time, Pallas kernels for 0%

profile of v1, /device:TPU:0, one launch (start us, length us, event | category | flops | bytes accessed | tf_op | source)
XLA Modules:
  0.0 408.1 jit_solution(12698315046776235370)
XLA Ops:
  6.6 1.1 copy.59
  8.0 1.1 copy.57
  9.9 11.3 %while.39 = (s32[]{:T(128)}, f32[2,128,128]{2,1,0:T(8,128)S(1)}, f32[2,128]{1,0:T(2,128)S(1)}, f32[2]{0:T(128)S(1)}, f32[2,2,256,128]{3,2,0,1:T(8,128)S(1)}, /*i...) while((s32[]{:T(128)}, f32[2,128,128]{2,1,0:T(8,128)S(1)}, ...), condition=%wide.region_6.7_spmd.clone, body=%wide.region_0.6_spmd.clone.sunk | while | flops 607329536 | bytes 4625314 | solution.py:116
  9.9 0.6 reduce-window.38
  11.4 0.2 fusion.122
  11.7 0.6 fusion.123
  12.4 0.2 fusion.121
  12.7 0.3 fusion.124
  13.3 0.4 convolution_multiply_fusion.4
  13.6 1.0 fusion.125
  14.8 0.7 convolution_add_fusion.3
  15.6 0.6 reduce-window.38
  17.0 0.2 fusion.122
  17.3 0.6 fusion.123
  18.0 0.2 fusion.121
  18.4 0.3 fusion.124
  18.9 0.4 convolution_multiply_fusion.4
  19.3 1.0 fusion.125
  20.4 0.7 convolution_add_fusion.3
  21.2 0.6 copy-done
  21.9 0.7 all-gather.14.cloned.1.call-update
  22.7 0.6 reduce-window.22
  23.9 0.7 dynamic-slice
  25.3 0.2 dynamic-update-slice.1
  25.6 23.3 %all-reduce.4 = (f32[16]{0:T(128)S(1)}, f32[16]{0:T(128)S(1)}) all-reduce(f32[16]{0:T(128)S(1)} %bitcast_dynamic-update-slice_fusion.1, f32[16]{0:T(128)S(1)} %dynamic-update-slice.1), channel_id=2, replica_groups=mesh['sp'=8,'tp'=4] {'sp'}, use_global_device_ids=true, to_apply=%add.1 | all-reduce | flops 32 | bytes 256
  49.0 16.4 %all-gather.5 = f32[8,2,128]{2,1,0:T(2,128)S(1)} all-gather(f32[1,2,128]{2,1,0:T(2,128)S(1)} %bitcast.297), channel_id=5, replica_groups=mesh['sp'=8,'tp'=4] {'sp'}, dimensions={0}, use_global_device_ids=true | all-gather | bytes 9216 | tf_op jit(solution)/shard_map/all_gather | solution.py:13
  65.5 9.0 %while.40 = (s32[]{:T(128)}, f32[2,128,128]{2,1,0:T(8,128)S(1)}, f32[2,128]{1,0:T(2,128)S(1)}, f32[2]{0:T(128)S(1)}, s32[]{:T(128)}, /*index=5*/f32[8,2]{1,0:T(8...) while((s32[]{:T(128)}, f32[2,128,128]{2,1,0:T(8,128)S(1)}, ...), condition=%wide.region_10.11_spmd.clone, body=%wide.region_9.10_spmd.clone.sunk | while | flops 165138 | bytes 396541 | solution.py:23
  65.5 1.0 fusion.126
  66.6 1.0 fusion.126
  67.7 1.0 fusion.126
  68.9 1.0 fusion.126
  70.0 1.0 fusion.126
  71.1 1.0 fusion.126
  72.2 1.0 fusion.126
  73.3 1.0 fusion.126
  74.4 0.4 fusion.66
  74.8 31.4 %all-gather.14.cloned.1.call-done = bf16[2048,256]{1,0:T(8,128)(2,1)} async-done(((bf16[256,256]{1,0:T(8,128)(2,1)}), bf16[2048,256]{1,0:T(8,128)(2,1)}) %all-gather.14.cloned.1.call-update) | async-done | bytes 1048592 | tf_op jit(solution)/shard_map/all_gather | solution.py:169
  106.2 1.8 copy.126
  108.0 0.5 reshape_reshape.3
  108.7 0.2 bitcast_multiply_fusion.5
  108.9 1.2 fusion.47
  110.1 2.1 bitcast_convert_fusion
  112.2 0.7 broadcast_multiply_fusion
  113.3 0.6 reduce-window.26
  113.9 0.2 slice_reduce_fusion.2
  114.6 1.6 scatter_custom_fusion
  116.3 25.9 %reduce-scatter.3.cloned.1.call-done = bf16[128,2048]{1,0:T(8,128)(2,1)} async-done(((bf16[512,2048]{1,0:T(8,128)(2,1)}), bf16[128,2048]{1,0:T(8,128)(2,1)}) %reduce-scatter.3.cloned.1.call-update) | async-done | bytes 524304 | tf_op jit(solution)/shard_map/reduce_scatter | solution.py:174
  142.2 1.3 fusion.48
  143.6 1.3 fusion.50
  144.9 2.4 gather_fusion
  147.3 36.6 %all_to_all.10 = bf16[8,1,40,2048]{3,2,1,0:T(8,128)(2,1)} all-to-all(bf16[8,1,40,2048]{3,2,1,0:T(8,128)(2,1)S(1)} %bitcast.278), channel_id=1, replica_groups=mesh['sp'=8,'tp'=4] {'sp'}, dimensions={0} | all-to-all | bytes 2621440 | tf_op jit(solution)/shard_map/all_to_all | solution.py:196
  184.0 38.6 %all-gather.10.cloned.1.call-done = bf16[8,4,40,2048]{3,2,1,0:T(8,128)(2,1)} async-done(((bf16[8,1,40,2048]{3,2,1,0:T(8,128)(2,1)}), bf16[8,4,40,2048]{3,2,1,0:T(8,128)(2,1)}) %all-gather.10.cloned.1.call-update) | async-done | bytes 5242896 | tf_op jit(solution)/shard_map/all_gather | solution.py:195
  222.6 10.0 %fusion.43 = f32[1280,896]{1,0:T(8,128)} fusion(bf16[1280,2048]{1,0:T(8,128)(2,1)} %bitcast.306, bf16[1,2048,896]{2,1,0:T(8,128)(2,1)} %param.27), kind=kOutput, calls=%fused_computation.81 | convolution fusion | flops 4697620480 | bytes 13500416 | tf_op jit(solution)/shard_map/dot_general | solution.py:209
  232.6 17.6 %convolution_convert_fusion = bf16[1280,2048]{1,0:T(8,128)(2,1)} fusion(bf16[1,896,2048]{2,1,0:T(8,128)(2,1)} %param.29, f32[1280,896]{1,0:T(8,128)} %fusion.43, bf16[1280,2048]{1,0:T(8,128)(2,1)} %bitcast.307, bf16[1,2048,896]{2,1,0:T(8,128)(2,1)} %param.28), kind=kOutput, calls=%fused_computation.76 | convolution fusion | flops 9404743680 | bytes 22413312 | tf_op jit(solution)/shard_map/dot_general | solution.py:212
  250.2 0.6 copy-done.11
  250.8 0.6 dynamic-slice.2
  251.4 101.5 %all-reduce.7.cloned.1.call-done = bf16[8,4,40,2048]{3,2,1,0:T(8,128)(2,1)} async-done(((bf16[8,4,40,2048]{3,2,1,0:T(8,128)(2,1)}), bf16[8,4,40,2048]{3,2,1,0:T(8,128)(2,1)}) %all-reduce.7.cloned.1.call-update) | async-done | bytes 5242896
  352.9 3.2 constant_dynamic-slice_fusion.3
  356.1 5.5 %all-to-all-start.1 = ((bf16[8,1,40,2048]{3,2,1,0:T(8,128)(2,1)}), bf16[8,1,40,2048]{3,2,1,0:T(8,128)(2,1)S(1)}, u32[]{:S(2)}, u32[]{:S(2)}) async-start(bf16[8,1,40,2048]{3,2,1,0:T(8,128)(2,1)} %constant_dynamic-slice_fusion.3), calls=%async_computation.2 | async-start | bytes 2621440 | tf_op jit(solution)/shard_map/all_to_all | solution.py:220
  361.7 30.9 %all-to-all-done.1 = bf16[8,1,40,2048]{3,2,1,0:T(8,128)(2,1)S(1)} async-done(((bf16[8,1,40,2048]{3,2,1,0:T(8,128)(2,1)}), bf16[8,1,40,2048]{3,2,1,0:T(8,128)(2,1)S(1)}, u32[]{:S(2)}, u32[]{:S(2)}) %all-to-all-start.1) | async-done | bytes 1310752 | tf_op jit(solution)/shard_map/all_to_all | solution.py:220
  392.6 2.3 gather_fusion.1
  395.0 2.4 reshape.428
  397.4 3.2 multiply_reduce_fusion
  400.6 1.0 fusion.51
  (143 shorter events, 6.9 us)
Async XLA Ops:
  6.5 2.9 copy-start.5
  6.5 3.3 copy-start.9
  6.5 3.3 copy-start.8
  6.5 3.3 copy-start.6
  6.5 58.9 %all-gather.12.cloned.1.call-start = ((), (), s32[]{:S(2)}) async-start(), calls=%async_computation.5 | async-start | bytes 1179648 | tf_op jit(solution)/shard_map/all_gather | solution.py:13
  9.9 14.1 %copy-start.12 = (u32[32]{0:T(128)S(1)}, u32[32]{0:T(128)}, u32[]{:S(2)}) copy-start(u32[32]{0:T(128)} %constant.125) | copy-start | bytes 388
  21.2 0.7 copy-start
  21.2 1.5 copy-start.3
  21.8 84.4 %all-gather.14.cloned.1.call-start = ((), (), s32[]{:S(2)}) async-start(), calls=%async_computation.6 | async-start | bytes 1179648 | tf_op jit(solution)/shard_map/all_gather | solution.py:169
  22.6 119.7 %reduce-scatter.3.cloned.1.call-start = ((), (), s32[]{:S(2)}) async-start(), calls=%async_computation.3 | async-start | bytes 2621440 | tf_op jit(solution)/shard_map/reduce_scatter | solution.py:174
  22.7 86.0 %copy-start.4 = (f32[2,2,256,128]{3,2,0,1:T(8,128)S(1)}, f32[2,2,256,128]{3,2,0,1:T(8,128)}, u32[]{:S(2)}) copy-start(f32[2,2,256,128]{3,2,0,1:T(8,128)} %copy-done.3) | copy-start | bytes 1572868
  108.9 33.3 %copy-start.1 = (bf16[128,2048]{1,0:T(8,128)(2,1)S(1)}, bf16[128,2048]{1,0:T(8,128)(2,1)}, u32[]{:S(2)}) copy-start(bf16[128,2048]{1,0:T(8,128)(2,1)} %param.24) | copy-start | bytes 1572868
  110.1 33.5 %copy-start.7 = (f32[2048]{0:T(1024)S(1)}, f32[2048]{0:T(1024)}, u32[]{:S(2)}) copy-start(f32[2048]{0:T(1024)} %param.26) | copy-start | bytes 24580
  112.2 110.4 %all-gather.10.cloned.1.call-start = ((), (), s32[]{:S(2)}) async-start(), calls=%async_computation.4 | async-start | bytes 6553600 | tf_op jit(solution)/shard_map/all_gather | solution.py:195
  184.0 168.9 %all-reduce.7.cloned.1.call-start = ((), (), s32[]{:S(2)}) async-start(), calls=%async_computation.7 | async-start | bytes 10485760
  250.1 0.7 copy-start.11
  250.2 111.4 %copy-start.10 = (f32[128,2]{0,1:T(2,128)S(1)}, f32[128,2]{0,1:T(2,128)}, u32[]{:S(2)}) copy-start(f32[128,2]{0,1:T(2,128)} %param.31) | copy-start | bytes 3076
  356.1 36.5 %all-to-all-start.1 = ((bf16[8,1,40,2048]{3,2,1,0:T(8,128)(2,1)}), bf16[8,1,40,2048]{3,2,1,0:T(8,128)(2,1)S(1)}, u32[]{:S(2)}, u32[]{:S(2)}) async-start(bf16[8,1,40,2048]{3,2,1,0:T(8,128)(2,1)} %constant_dynamic-slice_fusion.3), calls=%async_computation.2 | async-start | bytes 2621440 | tf_op jit(solution)/shard_map/all_to_all | solution.py:220
  395.0 5.6 %copy-start.2 = (bf16[128,2048]{1,0:T(8,128)(2,1)S(1)}, bf16[128,2048]{1,0:T(8,128)(2,1)}, u32[]{:S(2)}) copy-start(bf16[128,2048]{1,0:T(8,128)(2,1)} %reduce-scatter.3.cloned.1.call-done) | copy-start | bytes 1572868
Sparse Core Ops, SparseCore 0:
  22.0 43.0 all-gather.11
  67.2 38.9 all-gather.13
  112.3 29.8 reduce-scatter.2
  184.1 38.4 all-gather.9
  250.3 102.5 all-reduce.6
